TPU v7x, 32 devices: a whole 2x2x4 slice. The times are simulated.
32 devices in a mesh: sp: 8 (over z, y), tp: 4 (over x, core).
Axes of the slice: x: 2, y: 2, z: 4, core: 2. Of those that a mesh axis runs over, the one named last changes fastest.
Arguments:
- grad_out: bfloat16 [2048, 2048], P('sp'), may hold values from -6 to 6
- resid: bfloat16 [2048, 2048], P('sp'), may hold values from -6 to 6
- norm_gain: float32 [2048], replicated, may hold values from 0.1 to 1.9
- routes: int32 [2048, 2], P('sp'), may hold values from 0 to 7, all different within a row; in each aligned block of 256 rows (0 to 255, 256 to 511, ...) at most 96 rows name the same one
- route_weights: float32 [2048, 2], P('sp'), may hold values from 0.05 to 1
- gate_weight: bfloat16 [8, 2048, 1536], P('sp', None, 'tp'), may hold values from -0.375 to 0.375
- up_weight: bfloat16 [8, 2048, 1536], P('sp', None, 'tp'), may hold values from -0.375 to 0.375
- down_weight: bfloat16 [8, 1536, 2048], P('sp', 'tp'), may hold values from -0.15625 to 0.15625
- proj_weight: bfloat16 [2048, 512], P(None, 'tp'), may hold values from -0.25 to 0.25
- conv_sum: bfloat16 [2048, 512], P('sp', 'tp'), may hold values from -6 to 6
- conv_gain: float32 [512], P('tp'), may hold values from 0.1 to 1.9
- conv_taps: float32 [31, 512], P(None, 'tp'), may hold values from -1 to 1
- conv_value: bfloat16 [2048, 512], P('sp', 'tp'), may hold values from -6 to 6
- conv_gate: bfloat16 [2048, 512], P('sp', 'tp'), may hold values from -6 to 6
Outputs:
- gate_weight_grad: bfloat16 [8, 2048, 1536], P('sp', None, 'tp')
- up_weight_grad: bfloat16 [8, 2048, 1536], P('sp', None, 'tp')
- down_weight_grad: bfloat16 [8, 1536, 2048], P('sp', 'tp')
- proj_grad: float32 [2048, 512], P('sp', 'tp')
- value_grad: bfloat16 [2048, 512], P('sp', 'tp')
- gate_input_grad: bfloat16 [2048, 512], P('sp', 'tp')
Inputs may be any that keep to these rules, and one draw needn't show every extreme that they name: In each aligned block of 256 tokens no expert is named by more than 96 routes, and in some block one expert is named exactly 96 times; a token's two routes name different experts.
All inputs are finite; a program needn't handle non-finite values.
Results may differ from a plain program's by a relative error of at most 0.028.
Values may be sent and summed in bfloat16 or wider, within the bound.
No kernel may reach another device: no remote copies, remote signals or barrier semaphores. Data moves between devices by JAX's collectives and lax.ppermute only.
A program may use at most 128 MiB of HBM per device.

v0:
```python
import jax
import jax.numpy as jnp
from jax import lax
from jax.sharding import PartitionSpec as P

CONV_K = 31
GROUP = 128


CLAMP_LIMIT = 7.0
SLOPE_ALPHA = 1.702


def passed_along(block, axis, distance):
    devices = range(lax.axis_size(axis))
    route = [(i - distance, i) for i in devices if i - distance in devices]
    return lax.ppermute(block, axis, route)


def contract_rows(left_side, right_side):
    return lax.dot_general(
        left_side, right_side, (((0,), (0,)), ((), ())), preferred_element_type=jnp.float32
    )


def contract_cols(left_side, right_side):
    return lax.dot_general(
        left_side, right_side, (((1,), (1,)), ((), ())), preferred_element_type=jnp.float32
    )


def expert_backward(routed_rows, routed_cots, w_gate, w_up, w_down):
    gate_pre = jnp.dot(routed_rows, w_gate, preferred_element_type=jnp.float32)
    up_pre = jnp.dot(routed_rows, w_up, preferred_element_type=jnp.float32)
    gate_clamped = jnp.minimum(gate_pre, CLAMP_LIMIT)
    up_clamped = jnp.clip(up_pre, -CLAMP_LIMIT, CLAMP_LIMIT)
    sigma = jax.nn.sigmoid(SLOPE_ALPHA * gate_clamped)
    gated = gate_clamped * sigma
    act = ((up_clamped + 1.0) * gated).astype(jnp.bfloat16)
    down_grad = contract_rows(act, routed_cots).astype(jnp.bfloat16)
    act_grad = contract_cols(routed_cots, w_down)
    inside = (up_pre > -CLAMP_LIMIT) & (up_pre < CLAMP_LIMIT)
    up_pre_grad = jnp.where(inside, act_grad * gated, 0.0).astype(jnp.bfloat16)
    slope = sigma + SLOPE_ALPHA * gate_clamped * sigma * (1.0 - sigma)
    gate_pre_grad = jnp.where(
        gate_pre < CLAMP_LIMIT, act_grad * (up_clamped + 1.0) * slope, 0.0
    ).astype(jnp.bfloat16)
    gate_grad = contract_rows(routed_rows, gate_pre_grad).astype(jnp.bfloat16)
    up_grad = contract_rows(routed_rows, up_pre_grad).astype(jnp.bfloat16)
    partial_value = contract_cols(gate_pre_grad, w_gate) + contract_cols(up_pre_grad, w_up)
    return (gate_grad, up_grad, down_grad, partial_value)


def local(
    grad_out,
    resid,
    norm_gain,
    routes,
    route_weights,
    gate_weight,
    up_weight,
    down_weight,
    proj_weight,
    conv_sum,
    conv_gain,
    conv_taps,
    conv_value,
    conv_gate,
):
    tok_rows, model_width = resid.shape
    sp_count = lax.axis_size("sp")
    tp_count = lax.axis_size("tp")
    capacity = 3 * tok_rows // sp_count
    col_count = model_width // tp_count
    resid_f = resid.astype(jnp.float32)
    inv_rms = lax.rsqrt(jnp.mean(resid_f * resid_f, axis=-1, keepdims=True) + 1e-06)
    normed = (resid_f * inv_rms * norm_gain).astype(jnp.bfloat16)
    scaled = (route_weights[:, :, None] * grad_out.astype(jnp.float32)[:, None, :]).astype(
        jnp.bfloat16
    )
    scaled = scaled.reshape(2 * tok_rows, model_width)
    route_ids = routes.reshape(-1)
    one_hot = (route_ids[:, None] == jnp.arange(sp_count, dtype=jnp.int32)[None, :]).astype(
        jnp.int32
    )
    slot_rank = jnp.sum(jnp.cumsum(one_hot, axis=0) * one_hot, axis=1) - 1
    slot_index = route_ids * capacity + slot_rank
    slot_table = jnp.full((sp_count * capacity,), 2 * tok_rows, jnp.int32)
    slot_table = slot_table.at[slot_index].set(jnp.arange(2 * tok_rows, dtype=jnp.int32))
    normed_pad = jnp.concatenate([normed, jnp.zeros((1, model_width), jnp.bfloat16)], axis=0)
    scaled_pad = jnp.concatenate([scaled, jnp.zeros((1, model_width), jnp.bfloat16)], axis=0)
    first_col = lax.axis_index("tp") * col_count
    normed_part = lax.dynamic_slice_in_dim(normed_pad, first_col, col_count, 1)
    scaled_part = lax.dynamic_slice_in_dim(scaled_pad, first_col, col_count, 1)
    send_rows = normed_part[slot_table // 2].reshape(sp_count, capacity, col_count)
    send_cots = scaled_part[slot_table].reshape(sp_count, capacity, col_count)
    part_rows, part_cots = (
        lax.all_to_all(send_rows, "sp", split_axis=0, concat_axis=0, tiled=True),
        lax.all_to_all(send_cots, "sp", split_axis=0, concat_axis=0, tiled=True),
    )
    routed_rows, routed_cots = (
        lax.all_gather(part_rows, "tp", axis=2, tiled=True),
        lax.all_gather(part_cots, "tp", axis=2, tiled=True),
    )
    routed_rows = routed_rows.reshape(sp_count * capacity, model_width)
    routed_cots = routed_cots.reshape(sp_count * capacity, model_width)
    gate_grad, up_grad, down_grad, partial_value = expert_backward(
        routed_rows, routed_cots, gate_weight[0], up_weight[0], down_weight[0]
    )
    row_grad = lax.psum_scatter(
        partial_value.reshape(sp_count, capacity, model_width).astype(jnp.bfloat16),
        "tp",
        scatter_dimension=2,
        tiled=True,
    )
    returned = lax.all_to_all(row_grad, "sp", split_axis=0, concat_axis=0, tiled=True).reshape(
        sp_count * capacity, col_count
    )
    normed_part_grad = returned[slot_index].reshape(tok_rows, 2, col_count).astype(jnp.float32)
    normed_part_grad = normed_part_grad.sum(axis=1).astype(jnp.bfloat16)
    normed_grad = lax.all_gather(normed_part_grad, "tp", axis=1, tiled=True)
    feature_grad = normed_grad.astype(jnp.float32) * norm_gain
    cubed = inv_rms * inv_rms * inv_rms
    resid_grad = (
        grad_out.astype(jnp.float32)
        + inv_rms * feature_grad
        - resid_f * cubed * jnp.mean(resid_f * feature_grad, axis=-1, keepdims=True)
    ).astype(jnp.bfloat16)
    channels = conv_sum.shape[1]
    summed = conv_sum.astype(jnp.float32).reshape(tok_rows, channels // GROUP, GROUP)
    centre = summed - jnp.mean(summed, axis=-1, keepdims=True)
    inv_std = lax.rsqrt(jnp.mean(centre * centre, axis=-1, keepdims=True) + 1e-05)
    grouped = centre * inv_std
    chan_normed = grouped.reshape(tok_rows, channels)
    pre_act = chan_normed * conv_gain
    sigma_conv = jax.nn.sigmoid(pre_act)
    conv_out = (pre_act * sigma_conv).astype(jnp.bfloat16)
    proj_grad = lax.psum_scatter(
        contract_rows(resid_grad, conv_out), "sp", scatter_dimension=0, tiled=True
    )
    out_grad = jnp.dot(resid_grad, proj_weight, preferred_element_type=jnp.float32)
    normal_grad = (
        out_grad * sigma_conv * (1.0 + pre_act * (1.0 - sigma_conv)) * conv_gain
    ).reshape(tok_rows, channels // GROUP, GROUP)
    sum_grad = inv_std * (
        normal_grad
        - jnp.mean(normal_grad, axis=-1, keepdims=True)
        - grouped * jnp.mean(normal_grad * grouped, axis=-1, keepdims=True)
    )
    sum_grad = sum_grad.reshape(tok_rows, channels)
    following = passed_along(sum_grad[: CONV_K - 1], "sp", -1)
    extended = jnp.concatenate([sum_grad, following], axis=0)
    gated_grad = lax.conv_general_dilated(
        extended[None],
        conv_taps[::-1][:, None, :],
        (1,),
        ((0, 0),),
        dimension_numbers=("NWC", "WIO", "NWC"),
        feature_group_count=channels,
        precision=lax.Precision.HIGHEST,
    )[0]
    sigma_gate = jax.nn.sigmoid(conv_gate.astype(jnp.float32))
    value_grad = (gated_grad * sigma_gate).astype(jnp.bfloat16)
    gate_input_grad = (
        gated_grad * conv_value.astype(jnp.float32) * sigma_gate * (1.0 - sigma_gate)
    ).astype(jnp.bfloat16)
    return (gate_grad[None], up_grad[None], down_grad[None], proj_grad, value_grad, gate_input_grad)


def solution(mesh):
    in_specs = (
        P("sp", None),
        P("sp", None),
        P(),
        P("sp", None),
        P("sp", None),
        P("sp", None, "tp"),
        P("sp", None, "tp"),
        P("sp", "tp", None),
        P(None, "tp"),
        P("sp", "tp"),
        P("tp"),
        P(None, "tp"),
        P("sp", "tp"),
        P("sp", "tp"),
    )
    out_specs = (
        P("sp", None, "tp"),
        P("sp", None, "tp"),
        P("sp", "tp", None),
        P("sp", "tp"),
        P("sp", "tp"),
        P("sp", "tp"),
    )
    return jax.shard_map(local, mesh=mesh, in_specs=in_specs, out_specs=out_specs, check_vma=False)
```

profile of v0, /device:TPU:0, one launch (start us, length us, event | category | flops | bytes accessed | tf_op | source)
XLA Modules:
  0.0 286.5 jit_solution(7567787872542346004)
XLA Ops:
  7.3 0.8 broadcast_multiply_fusion
  8.1 0.8 copy.25
  8.9 0.1 eq.29
  9.2 1.5 fusion.3
  10.9 0.1 mul.210
  11.0 1.1 reduce-window.6
  12.2 0.2 slice_reduce_fusion
  12.6 2.4 scatter_custom_fusion
  15.0 0.3 fusion.5
  15.4 3.3 %gather_fusion = bf16[768,512]{1,0:T(8,128)(2,1)} fusion(bf16[257,512]{1,0:T(8,128)(2,1)S(1)} %pad_dynamic-slice_fusion.1, s32[1024]{0:T(1024)S(1)} %get-tuple-element.18), kind=kCustom, calls=%fused_computation | custom fusion | bytes 1575936 | tf_op jit(solution)/shard_map/gather | solution.py:95
  18.7 27.6 %all_to_all.15 = bf16[8,96,512]{2,1,0:T(8,128)(2,1)} all-to-all(bf16[8,96,512]{2,1,0:T(8,128)(2,1)} %bitcast.63), channel_id=1, replica_groups=mesh['sp'=8,'tp'=4] {'sp'}, dimensions={0} | all-to-all | bytes 1572864 | tf_op jit(solution)/shard_map/all_to_all | solution.py:98
  46.4 5.3 %mul.214 = f32[256,2,2048]{2,1,0:T(2,128)} broadcast(bf16[256,2048]{1,0:T(8,128)(2,1)} %param.14), dimensions={0,2} | broadcast | bytes 5242880 | tf_op jit(solution)/shard_map/mul | solution.py:78
  51.7 6.2 %mul.215 = f32[512,2048]{1,0:T(8,128)} reshape(f32[256,2,2048]{2,1,0:T(2,128)} %mul.214) | data formatting | bytes 8388608 | tf_op jit(solution)/shard_map/mul | solution.py:78
  58.0 0.1 mul.212
  58.1 2.5 multiply_convert_fusion
  60.7 3.3 %gather_fusion.1 = bf16[768,512]{1,0:T(8,128)(2,1)} fusion(bf16[513,512]{1,0:T(8,128)(2,1)S(1)} %pad_dynamic-slice_fusion, s32[1024]{0:T(1024)S(1)} %get-tuple-element.17), kind=kCustom, calls=%fused_computation.1 | custom fusion | bytes 1575936 | tf_op jit(solution)/shard_map/gather | solution.py:96
  64.0 23.7 %all_to_all.16 = bf16[8,96,512]{2,1,0:T(8,128)(2,1)} all-to-all(bf16[8,96,512]{2,1,0:T(8,128)(2,1)} %bitcast.64), channel_id=1, replica_groups=mesh['sp'=8,'tp'=4] {'sp'}, dimensions={0} | all-to-all | bytes 1572864 | tf_op jit(solution)/shard_map/all_to_all | solution.py:99
  87.7 0.2 reduce-scatter.3.cloned.1.call-start
  88.0 5.3 %fusion.11 = f32[768,384]{1,0:T(8,128)} fusion(bf16[768,2048]{1,0:T(8,128)(2,1)} %bitcast.70, bf16[1,2048,384]{2,1,0:T(8,128)(2,1)} %param.20), kind=kOutput, calls=%fused_computation.26 | convolution fusion | flops 1207959552 | bytes 5898240 | tf_op jit(solution)/shard_map/dot_general | solution.py:34
  93.3 2.8 fusion.17
  96.1 19.2 %all-gather.6.cloned.1.call-done = bf16[8,96,2048]{2,1,0:T(8,128)(2,1)} async-done(((bf16[8,96,512]{2,1,0:T(8,128)(2,1)}), bf16[8,96,2048]{2,1,0:T(8,128)(2,1)}) %all-gather.6.cloned.1.call-update) | async-done | bytes 3145744 | tf_op jit(solution)/shard_map/all_gather | solution.py:103
  115.3 5.5 %select_convert_fusion = (bf16[768,384]{1,0:T(8,128)(2,1)S(1)}, bf16[768,384]{1,0:T(8,128)(2,1)S(1)}) fusion(f32[768,384]{1,0:T(8,128)} %fusion.11, f32[768,384]{1,0:T(8,128)} %fusion.17, bf16[768,2048]{1,0:T(8,128)(2,1)} %bitcast.74, bf16[1,384,2048]{2,1,0:T(8,128)(2,1)} %param.21), kind=kOutput, calls=%fused_computation.35 | convolution fusion | flops 1214742528 | bytes 8257536 | tf_op jit(solution)/shard_map/dot_general | solution.py:27
  120.8 1.8 fusion.15
  122.7 3.5 %add_convert_fusion = bf16[768,2048]{1,0:T(8,128)(2,1)} fusion(f32[768,2048]{1,0:T(8,128)S(1)} %fusion.15, bf16[768,384]{1,0:T(8,128)(2,1)S(1)} %get-tuple-element.8, bf16[1,2048,384]{2,1,0:T(8,128)(2,1)S(1)} %copy-done.6), kind=kOutput, calls=%fused_computation.4 | convolution fusion | flops 1211105280 | bytes 11599872 | tf_op jit(solution)/shard_map/dot_general | solution.py:27
  126.2 37.9 %reduce-scatter.3.cloned.1.call-done = bf16[8,96,512]{2,1,0:T(8,128)(2,1)} async-done(((bf16[8,96,2048]{2,1,0:T(8,128)(2,1)}), bf16[8,96,512]{2,1,0:T(8,128)(2,1)}) %reduce-scatter.3.cloned.1.call-update) | async-done | bytes 786448 | tf_op jit(solution)/shard_map/reduce_scatter | solution.py:110
  164.1 5.5 %all-to-all-start.2 = ((bf16[8,96,512]{2,1,0:T(8,128)(2,1)}), bf16[8,96,512]{2,1,0:T(8,128)(2,1)S(1)}, u32[]{:S(2)}, u32[]{:S(2)}) async-start(bf16[8,96,512]{2,1,0:T(8,128)(2,1)} %reduce-scatter.3.cloned.1.call-done), calls=%async_computation.3 | async-start | bytes 1572864 | tf_op jit(solution)/shard_map/all_to_all | solution.py:116
  169.6 20.0 %all-to-all-done.2 = bf16[8,96,512]{2,1,0:T(8,128)(2,1)S(1)} async-done(((bf16[8,96,512]{2,1,0:T(8,128)(2,1)}), bf16[8,96,512]{2,1,0:T(8,128)(2,1)S(1)}, u32[]{:S(2)}, u32[]{:S(2)}) %all-to-all-start.2) | async-done | bytes 786464 | tf_op jit(solution)/shard_map/all_to_all | solution.py:116
  189.6 2.6 gather_fusion.2
  192.3 1.3 reshape.172
  193.5 2.1 reduce_sum.77
  195.7 0.3 reduce-scatter.5.cloned.1.call-start
  196.1 0.2 fusion.46
  196.3 5.3 %fusion.2 = bf16[1,384,2048]{2,1,0:T(8,128)(2,1)} fusion(bf16[768,2048]{1,0:T(8,128)(2,1)} %bitcast.75, f32[768,384]{1,0:T(8,128)} %fusion.11, f32[768,384]{1,0:T(8,128)} %fusion.17), kind=kOutput, calls=%fused_computation.15 | convolution fusion | flops 1211695104 | bytes 7077888 | tf_op jit(solution)/shard_map/dot_general | solution.py:21
  201.6 8.9 %all-gather.8.cloned.1.call-done = bf16[256,2048]{1,0:T(8,128)(2,1)} async-done(((bf16[256,512]{1,0:T(8,128)(2,1)}), bf16[256,2048]{1,0:T(8,128)(2,1)}) %all-gather.8.cloned.1.call-update) | async-done | bytes 1048592 | tf_op jit(solution)/shard_map/all_gather | solution.py:121
  210.5 1.8 fusion.9
  212.3 0.7 fusion.8
  213.1 1.0 copy-done.3
  214.0 1.5 fusion.47
  215.6 5.1 %fusion = bf16[1,2048,384]{2,1,0:T(8,128)(2,1)} fusion(bf16[768,2048]{1,0:T(8,128)(2,1)} %bitcast.71, bf16[768,384]{1,0:T(8,128)(2,1)} %copy-done.8), kind=kOutput, calls=%fused_computation.13 | convolution fusion | flops 1208745984 | bytes 5308416 | tf_op jit(solution)/shard_map/dot_general | solution.py:21
  220.8 0.6 fusion.67
  221.3 0.2 fusion.45
  221.6 1.3 collective-permute-start
  222.9 3.0 %fusion.1 = bf16[1,2048,384]{2,1,0:T(8,128)(2,1)} fusion(bf16[768,2048]{1,0:T(8,128)(2,1)S(1)} %bitcast.73, bf16[768,384]{1,0:T(8,128)(2,1)S(1)} %copy-done.10), kind=kOutput, calls=%fused_computation.14 | convolution fusion | flops 1208745984 | bytes 5308416 | tf_op jit(solution)/shard_map/dot_general | solution.py:21
  225.9 1.3 collective-permute-done
  227.3 0.3 convolution_select_fusion
  227.7 0.4 copy-done.12
  228.2 0.7 multiply_convert_fusion.3
  228.9 51.1 %reduce-scatter.5.cloned.1.call-done = f32[256,128]{1,0:T(8,128)} async-done(((f32[2048,128]{1,0:T(8,128)}), f32[256,128]{1,0:T(8,128)}) %reduce-scatter.5.cloned.1.call-update) | async-done | bytes 131088 | tf_op jit(solution)/shard_map/reduce_scatter | solution.py:138
  (79 shorter events, 1.3 us)
Async XLA Ops:
  7.2 86.1 %copy-start = (bf16[1,2048,384]{2,1,0:T(8,128)(2,1)S(1)}, bf16[1,2048,384]{2,1,0:T(8,128)(2,1)}, u32[]{:S(2)}) copy-start(bf16[1,2048,384]{2,1,0:T(8,128)(2,1)} %param.19) | copy-start | bytes 4718596
  7.2 7.8 %copy-start.1 = (bf16[256,2048]{1,0:T(8,128)(2,1)S(1)}, bf16[256,2048]{1,0:T(8,128)(2,1)}, u32[]{:S(2)}) copy-start(bf16[256,2048]{1,0:T(8,128)(2,1)} %param.15) | copy-start | bytes 3145732
  7.2 7.8 %copy-start.11 = (f32[2048]{0:T(1024)S(1)}, f32[2048]{0:T(1024)}, u32[]{:S(2)}) copy-start(f32[2048]{0:T(1024)} %param.16) | copy-start | bytes 24580
  7.2 80.8 %all-gather.4.cloned.1.call-start = ((), (), s32[]{:S(2)}) async-start(), calls=%async_computation.5 | async-start | bytes 3932160 | tf_op jit(solution)/shard_map/all_gather | solution.py:102
  46.3 69.0 %all-gather.6.cloned.1.call-start = ((), (), s32[]{:S(2)}) async-start(), calls=%async_computation.6 | async-start | bytes 3932160 | tf_op jit(solution)/shard_map/all_gather | solution.py:103
  51.7 6.2 %copy-start.15 = (f32[256,2]{0,1:T(2,128)S(1)}, f32[256,2]{0,1:T(2,128)}, u32[]{:S(2)}) copy-start(f32[256,2]{0,1:T(2,128)} %param.18) | copy-start | bytes 6148
  87.7 76.3 %reduce-scatter.3.cloned.1.call-start = ((), (), s32[]{:S(2)}) async-start(), calls=%async_computation.7 | async-start | bytes 3932160 | tf_op jit(solution)/shard_map/reduce_scatter | solution.py:110
  88.0 5.3 %copy-start.17 = (bf16[8,96,2048]{2,1,0:T(8,128)(2,1)S(1)}, bf16[8,96,2048]{2,1,0:T(8,128)(2,1)}, u32[]{:S(2)}) copy-start(bf16[8,96,2048]{2,1,0:T(8,128)(2,1)} %all-gather.4.cloned.1.call-done) | copy-start | bytes 9437188
  120.8 1.9 copy-start.8
  120.8 1.9 copy-start.9
  120.8 1.9 copy-start.6
  164.1 25.6 %all-to-all-start.2 = ((bf16[8,96,512]{2,1,0:T(8,128)(2,1)}), bf16[8,96,512]{2,1,0:T(8,128)(2,1)S(1)}, u32[]{:S(2)}, u32[]{:S(2)}) async-start(bf16[8,96,512]{2,1,0:T(8,128)(2,1)} %reduce-scatter.3.cloned.1.call-done), calls=%async_computation.3 | async-start | bytes 1572864 | tf_op jit(solution)/shard_map/all_to_all | solution.py:116
  169.6 40.9 %all-gather.8.cloned.1.call-start = ((), (), s32[]{:S(2)}) async-start(), calls=%async_computation.8 | async-start | bytes 1310720 | tf_op jit(solution)/shard_map/all_gather | solution.py:121
  192.3 3.7 %copy-start.14 = (f32[31,128]{1,0:T(8,128)S(1)}, f32[31,128]{1,0:T(8,128)}, u32[]{:S(2)}) copy-start(f32[31,128]{1,0:T(8,128)} %param.25) | copy-start | bytes 47620
  192.3 3.7 %copy-start.7 = (bf16[256,128]{1,0:T(8,128)(2,1)S(1)}, bf16[256,128]{1,0:T(8,128)(2,1)}, u32[]{:S(2)}) copy-start(bf16[256,128]{1,0:T(8,128)(2,1)} %param.23) | copy-start | bytes 196612
  195.7 84.3 %reduce-scatter.5.cloned.1.call-start = ((), (), s32[]{:S(2)}) async-start(), calls=%async_computation.9 | async-start | bytes 1179648 | tf_op jit(solution)/shard_map/reduce_scatter | solution.py:138
  210.5 1.8 copy-start.2
  210.5 1.9 copy-start.5
  212.3 1.7 copy-start.16
  213.1 1.0 copy-start.3
  215.6 5.2 %copy-start.4 = (bf16[256,2048]{1,0:T(8,128)(2,1)S(1)}, bf16[256,2048]{1,0:T(8,128)(2,1)}, u32[]{:S(2)}) copy-start(bf16[256,2048]{1,0:T(8,128)(2,1)} %copy-done.3) | copy-start | bytes 3145732
  215.6 5.2 %copy-start.19 = (bf16[2048,128]{1,0:T(8,128)(2,1)S(1)}, bf16[2048,128]{1,0:T(8,128)(2,1)}, u32[]{:S(2)}) copy-start(bf16[2048,128]{1,0:T(8,128)(2,1)} %param.22) | copy-start | bytes 1572868
  215.6 7.3 %copy-start.18 = (bf16[8,96,2048]{2,1,0:T(8,128)(2,1)S(1)}, bf16[8,96,2048]{2,1,0:T(8,128)(2,1)}, u32[]{:S(2)}) copy-start(bf16[8,96,2048]{2,1,0:T(8,128)(2,1)} %all-gather.4.cloned.1.call-done) | copy-start | bytes 9437188
  220.8 2.1 copy-start.10
  221.6 5.7 %copy-start.20 = (pred[8,36]{0,1:T(8,128)(4,1)S(1)}, pred[8,36]{0,1:T(8,128)(4,1)}, u32[]{:S(2)}) copy-start(pred[8,36]{0,1:T(8,128)(4,1)} %constant.83) | copy-start | bytes 868
  221.6 5.6 %collective-permute-start = (f32[30,128]{1,0:T(8,128)S(1)}, f32[30,128]{1,0:T(8,128)S(1)}, u32[]{:S(2)}, u32[]{:S(2)}) collective-permute-start(f32[30,128]{1,0:T(8,128)S(1)} %slice.23), channel_id=1, source_target_pairs={{4,0},{8,4},{12,8},{16,12},{20,16},{24,20},{28,24},{5,1},{9,5},{13... | collective-permute-start | bytes 46088 | tf_op jit(solution)/shard_map/ppermute | solution.py:17
  227.3 0.8 copy-start.12
  227.3 0.9 copy-start.13
Sparse Core Ops, SparseCore 0:
  46.4 27.4 all-gather.3
  87.8 27.3 all-gather.5
  126.3 37.7 reduce-scatter.2
  195.8 14.6 all-gather.7
  215.7 64.2 reduce-scatter.4
where the time goes:
time: 287 us; the launch traced here: 286 us
  waiting for transfers between devices  138 us (48%)
  blocking collectives  51.2 us (18%)
  matrix products  34.8 us (12%)
  local copies, waits for them, and re-layouts  28.1 us (10%)
  between operations  14.2 us (5%)
  other arithmetic  12.3 us (4%)
  starting transfers between devices  7.41 us (3%)
    reduce_scatter x1, waiting for transfers between devices, local(): lax.psum_scatter(contract_rows(resid_grad, conv_out), 'sp', scatter_dimen...  51.1 us
    reduce_scatter x1, waiting for transfers between devices, local(): lax.psum_scatter(partial_value.reshape(sp_count, capacity, model_width).a...  37.9 us
    all_to_all x1, blocking collectives, local(): lax.all_to_all(send_rows, 'sp', split_axis=0, concat_axis=0, tiled=True)  27.6 us
    all_to_all x1, blocking collectives, local(): lax.all_to_all(send_cots, 'sp', split_axis=0, concat_axis=0, tiled=True)  23.7 us
    all_to_all x1, waiting for transfers between devices, local(): lax.all_to_all(row_grad, 'sp', split_axis=0, concat_axis=0, tiled=True)  20 us
    all_gather x1, waiting for transfers between devices, local(): lax.all_gather(part_cots, 'tp', axis=2, tiled=True)  19.2 us
    dot_general x4, matrix products, contract_rows(): lax.dot_general(left_side, right_side, (((0,), (0,)), ((), ())), preferre...  15 us
    mul x3, local copies, waits for them, and re-layouts, local(): route_weights[:, :, None] * grad_out.astype(jnp.float32)[:, None, :]  11.6 us
  transfers between devices with their start and end apart: 7, of which 6 were waited for; matrix products, arithmetic and copies ran while one was open for 14% of the time, Pallas kernels for 0%

commit v1 on v0

v1 whole, which is shorter than its diff:
```python
import jax
import jax.numpy as jnp
from jax import lax
from jax.sharding import PartitionSpec as P

CONV_K = 31
GROUP = 128


CLAMP_LIMIT = 7.0
SLOPE_ALPHA = 1.702
SEND_CHUNKS = 2


def passed_along(block, axis, distance):
    devices = range(lax.axis_size(axis))
    route = [(i - distance, i) for i in devices if i - distance in devices]
    return lax.ppermute(block, axis, route)


def contract_rows(left_side, right_side):
    return lax.dot_general(
        left_side, right_side, (((0,), (0,)), ((), ())), preferred_element_type=jnp.float32
    )


def contract_cols(left_side, right_side):
    return lax.dot_general(
        left_side, right_side, (((1,), (1,)), ((), ())), preferred_element_type=jnp.float32
    )


def exchanged(block, axis, flip):
    route = [(i, i ^ flip) for i in range(lax.axis_size(axis))]
    return lax.ppermute(block, axis, route)


def swapped(blocks):
    return lax.all_to_all(blocks, "sp", split_axis=0, concat_axis=0, tiled=True)


def gather_cols(part, own, count):
    rows, width = part.shape
    parts = {0: part}
    bit = count >> 1
    while bit:
        for flip in sorted(parts):
            parts[flip | bit] = exchanged(parts[flip], "tp", bit)
        bit >>= 1
    full = jnp.zeros((rows, width * count), part.dtype)
    for flip in range(count):
        full = lax.dynamic_update_slice(full, parts[flip], (0, (own ^ flip) * width))
    return full


def scatter_cols(partial, own, count):
    width = partial.shape[1] // count
    parts = {
        flip: lax.dynamic_slice_in_dim(partial, (own ^ flip) * width, width, 1)
        for flip in range(count)
    }
    bit = 1
    while bit < count:
        sent = {}
        for flip in sorted(parts)[::-1]:
            if flip & bit:
                sent[flip] = exchanged(parts[flip], "tp", bit)
        parts = {
            flip: (
                parts[flip].astype(jnp.float32) + sent[flip | bit].astype(jnp.float32)
            ).astype(jnp.bfloat16)
            for flip in parts
            if not flip & bit
        }
        bit <<= 1
    return parts[0]


def backward(
    grad_out,
    resid,
    norm_gain,
    routes,
    route_weights,
    gate_weight,
    up_weight,
    down_weight,
    proj_weight,
    conv_sum,
    conv_gain,
    conv_taps,
    conv_value,
    conv_gate,
):
    tok_rows, model_width = resid.shape
    sp_count = lax.axis_size("sp")
    tp_count = lax.axis_size("tp")
    tp_own = lax.axis_index("tp")
    capacity = 3 * tok_rows // sp_count
    col_count = model_width // tp_count
    send_chunks = SEND_CHUNKS if capacity % (16 * SEND_CHUNKS) == 0 else 1
    piece = capacity // send_chunks
    first_col = tp_own * col_count
    w_gate, w_up, w_down = gate_weight[0], up_weight[0], down_weight[0]

    order = jnp.arange(sp_count, dtype=jnp.int32)
    named = routes.T[:, None, :] == order[None, :, None]
    member = named[0] | named[1]
    earlier = (
        jnp.arange(tok_rows, dtype=jnp.int32)[:, None] < jnp.arange(tok_rows, dtype=jnp.int32)[None, :]
    )
    rank = jnp.dot(
        member.astype(jnp.bfloat16), earlier.astype(jnp.bfloat16), preferred_element_type=jnp.float32
    ).astype(jnp.int32)
    rank = jnp.where(member, rank, -1)
    token_weight = jnp.sum(jnp.where(named, route_weights.T[:, None, :], 0.0), axis=0)
    hit = rank[:, None, :] == jnp.arange(capacity, dtype=jnp.int32)[None, :, None]
    chosen = hit.astype(jnp.bfloat16)
    slot_weight = jnp.sum(jnp.where(hit, token_weight[:, None, :], 0.0), axis=-1)

    resid_f = resid.astype(jnp.float32)
    inv_rms = lax.rsqrt(jnp.mean(resid_f * resid_f, axis=-1, keepdims=True) + 1e-06)
    resid_part = lax.dynamic_slice_in_dim(resid, first_col, col_count, 1).astype(jnp.float32)
    gain_part = lax.dynamic_slice_in_dim(norm_gain, first_col, col_count, 0)
    normed_part = (resid_part * inv_rms * gain_part).astype(jnp.bfloat16)
    cots_part = lax.dynamic_slice_in_dim(grad_out, first_col, col_count, 1)

    select = chosen.reshape(sp_count * capacity, tok_rows)

    def sent_out(value):
        return swapped(value.reshape(sp_count, -1, col_count))

    def pieces(value):
        return [
            value[:, chunk * piece : (chunk + 1) * piece].reshape(-1, col_count)
            for chunk in range(send_chunks)
        ]

    rows_out = jnp.dot(select, normed_part, preferred_element_type=jnp.float32)
    cots_out = jnp.dot(select, cots_part, preferred_element_type=jnp.float32)
    cots_out = cots_out * slot_weight.reshape(-1, 1)
    rows_in = pieces(sent_out(rows_out.astype(jnp.bfloat16)))
    cots_in = pieces(sent_out(cots_out.astype(jnp.bfloat16)))
    rows_full = [gather_cols(value, tp_own, tp_count) for value in rows_in]
    cots_full = [gather_cols(value, tp_own, tp_count) for value in cots_in]

    acts, gate_grads, up_grads, returned = [], [], [], []
    for routed_rows, routed_cots in zip(rows_full, cots_full):
        gate_pre = jnp.dot(routed_rows, w_gate, preferred_element_type=jnp.float32)
        up_pre = jnp.dot(routed_rows, w_up, preferred_element_type=jnp.float32)
        gate_clamped = jnp.minimum(gate_pre, CLAMP_LIMIT)
        up_clamped = jnp.clip(up_pre, -CLAMP_LIMIT, CLAMP_LIMIT)
        sigma = jax.nn.sigmoid(SLOPE_ALPHA * gate_clamped)
        gated = gate_clamped * sigma
        acts.append(((up_clamped + 1.0) * gated).astype(jnp.bfloat16))
        act_grad = contract_cols(routed_cots, w_down)
        inside = (up_pre > -CLAMP_LIMIT) & (up_pre < CLAMP_LIMIT)
        up_pre_grad = jnp.where(inside, act_grad * gated, 0.0).astype(jnp.bfloat16)
        slope = sigma + SLOPE_ALPHA * gate_clamped * sigma * (1.0 - sigma)
        gate_pre_grad = jnp.where(
            gate_pre < CLAMP_LIMIT, act_grad * (up_clamped + 1.0) * slope, 0.0
        ).astype(jnp.bfloat16)
        gate_grads.append(gate_pre_grad)
        up_grads.append(up_pre_grad)
        partial_value = contract_cols(gate_pre_grad, w_gate) + contract_cols(up_pre_grad, w_up)
        row_grad = scatter_cols(partial_value.astype(jnp.bfloat16), tp_own, tp_count)
        returned.append(sent_out(row_grad).reshape(-1, col_count))

    def weight_grad(lefts, rights):
        return sum(contract_rows(l, r) for l, r in zip(lefts, rights)).astype(jnp.bfloat16)

    down_grad = weight_grad(acts, cots_full)
    gate_grad = weight_grad(rows_full, gate_grads)
    up_grad = weight_grad(rows_full, up_grads)

    normed_part_grad = sum(
        contract_rows(
            chosen[:, chunk * piece : (chunk + 1) * piece].reshape(sp_count * piece, tok_rows),
            returned[chunk],
        )
        for chunk in range(send_chunks)
    ).astype(jnp.bfloat16)
    normed_grad = gather_cols(normed_part_grad, tp_own, tp_count)
    feature_grad = normed_grad.astype(jnp.float32) * norm_gain
    cubed = inv_rms * inv_rms * inv_rms
    resid_grad = (
        grad_out.astype(jnp.float32)
        + inv_rms * feature_grad
        - resid_f * cubed * jnp.mean(resid_f * feature_grad, axis=-1, keepdims=True)
    ).astype(jnp.bfloat16)
    channels = conv_sum.shape[1]
    summed = conv_sum.astype(jnp.float32).reshape(tok_rows, channels // GROUP, GROUP)
    centre = summed - jnp.mean(summed, axis=-1, keepdims=True)
    inv_std = lax.rsqrt(jnp.mean(centre * centre, axis=-1, keepdims=True) + 1e-05)
    grouped = centre * inv_std
    chan_normed = grouped.reshape(tok_rows, channels)
    pre_act = chan_normed * conv_gain
    sigma_conv = jax.nn.sigmoid(pre_act)
    conv_out = (pre_act * sigma_conv).astype(jnp.bfloat16)
    proj_term = contract_rows(resid_grad, conv_out).astype(jnp.bfloat16)
    terms = swapped(proj_term.reshape(sp_count, model_width // sp_count, channels))
    proj_grad = jnp.sum(terms.astype(jnp.float32), axis=0)
    out_grad = jnp.dot(resid_grad, proj_weight, preferred_element_type=jnp.float32)
    normal_grad = (
        out_grad * sigma_conv * (1.0 + pre_act * (1.0 - sigma_conv)) * conv_gain
    ).reshape(tok_rows, channels // GROUP, GROUP)
    sum_grad = inv_std * (
        normal_grad
        - jnp.mean(normal_grad, axis=-1, keepdims=True)
        - grouped * jnp.mean(normal_grad * grouped, axis=-1, keepdims=True)
    )
    sum_grad = sum_grad.reshape(tok_rows, channels)
    following = passed_along(sum_grad[: CONV_K - 1], "sp", -1)
    extended = jnp.concatenate([sum_grad, following], axis=0)
    gated_grad = lax.conv_general_dilated(
        extended[None],
        conv_taps[::-1][:, None, :],
        (1,),
        ((0, 0),),
        dimension_numbers=("NWC", "WIO", "NWC"),
        feature_group_count=channels,
        precision=lax.Precision.HIGHEST,
    )[0]
    sigma_gate = jax.nn.sigmoid(conv_gate.astype(jnp.float32))
    value_grad = (gated_grad * sigma_gate).astype(jnp.bfloat16)
    gate_input_grad = (
        gated_grad * conv_value.astype(jnp.float32) * sigma_gate * (1.0 - sigma_gate)
    ).astype(jnp.bfloat16)
    return (gate_grad[None], up_grad[None], down_grad[None], proj_grad, value_grad, gate_input_grad)


def solution(mesh):
    in_specs = (
        P("sp", None),
        P("sp", None),
        P(),
        P("sp", None),
        P("sp", None),
        P("sp", None, "tp"),
        P("sp", None, "tp"),
        P("sp", "tp", None),
        P(None, "tp"),
        P("sp", "tp"),
        P("tp"),
        P(None, "tp"),
        P("sp", "tp"),
        P("sp", "tp"),
    )
    out_specs = (
        P("sp", None, "tp"),
        P("sp", None, "tp"),
        P("sp", "tp", None),
        P("sp", "tp"),
        P("sp", "tp"),
        P("sp", "tp"),
    )
    return jax.shard_map(backward, mesh=mesh, in_specs=in_specs, out_specs=out_specs, check_vma=False)
```

time: 287 us -> 182 us (0.63)
  waiting for transfers between devices: 138 us -> 75 us
  blocking collectives: 51.2 us -> 0 us
  starting transfers between devices: 7.41 us -> 37.1 us
  local copies, waits for them, and re-layouts: 28.1 us -> 10.2 us
  between operations: 14.2 us -> 1.54 us
  matrix products: 34.8 us -> 43.5 us
    reduce_scatter x2 -> x0, waiting for transfers between devices: 88.9 us -> none  [the longest x1 51.1 us: local(): lax.psum_scatter(contract_rows(resid_grad, conv_out), 'sp', scatter_dimen...]
    all_to_all x2 -> x0, blocking collectives: 51.2 us -> none  [the longest x1 27.6 us: local(): lax.all_to_all(send_rows, 'sp', split_axis=0, concat_axis=0, tiled=True)]
    all_gather x3 -> x0, waiting for transfers between devices: 28.1 us -> none  [the longest x1 19.2 us: local(): lax.all_gather(part_cots, 'tp', axis=2, tiled=True)]
    ppermute x0 -> x21, waiting for transfers between devices: none -> 27.8 us  [exchanged(): return lax.ppermute(block, axis, route)]
    all_to_all x1 -> x5, waiting for transfers between devices: 20 us -> 46.1 us  [swapped(): return lax.all_to_all(blocks, 'sp', split_axis=0, concat_axis=0, tiled=True)]
    all_to_all x1 -> x5, starting transfers between devices: 5.52 us -> 25 us  [swapped(): return lax.all_to_all(blocks, 'sp', split_axis=0, concat_axis=0, tiled=True)]
    mul x5 -> x1, local copies, waits for them, and re-layouts: 11.9 us -> 0.07 us  [backward(): cots_out = cots_out * slot_weight.reshape(-1, 1)]
    dot_general x4 -> x9, matrix products: 15 us -> 26.8 us  [contract_rows(): lax.dot_general(left_side, right_side, (((0,), (0,)), ((), ())), preferre...]
  transfers between devices with their start and end apart: 7 -> 27, of which waited for: 6 -> 11; matrix products, arithmetic and copies ran while one was open for 14% -> 27% of each run, Pallas kernels for 0% -> 0%
where the time goes in v1:
time: 182 us; the launch traced here: 181 us
  waiting for transfers between devices  75 us (41%)
  matrix products  43.5 us (24%)
  starting transfers between devices  37.1 us (20%)
  other arithmetic  14 us (8%)
  local copies, waits for them, and re-layouts  10.2 us (6%)
    all_to_all x5, waiting for transfers between devices, swapped(): return lax.all_to_all(blocks, 'sp', split_axis=0, concat_axis=0, tiled=True)  46.1 us
    ppermute x21, waiting for transfers between devices, exchanged(): return lax.ppermute(block, axis, route)  27.8 us
    dot_general x9, matrix products, contract_rows(): lax.dot_general(left_side, right_side, (((0,), (0,)), ((), ())), preferre...  26.8 us
    all_to_all x5, starting transfers between devices, swapped(): return lax.all_to_all(blocks, 'sp', split_axis=0, concat_axis=0, tiled=True)  25 us
    ppermute x21, starting transfers between devices, exchanged(): return lax.ppermute(block, axis, route)  10.9 us
    dot_general x6, matrix products, contract_cols(): lax.dot_general(left_side, right_side, (((1,), (1,)), ((), ())), preferre...  6.6 us
    convert_element_type x4, other arithmetic, scatter_cols(): parts = {flip: (parts[flip].astype(jnp.float32) + sent[flip | bit].astype...  4.13 us
    dynamic_update_slice x19, local copies, waits for them, and re-layouts, gather_cols(): lax.dynamic_update_slice(full, parts[flip], (0, (own ^ flip) * width))  3.75 us
  transfers between devices with their start and end apart: 27, of which 11 were waited for; matrix products, arithmetic and copies ran while one was open for 27% of the time, Pallas kernels for 0%

profile of v1, /device:TPU:0, one launch (start us, length us, event | category | flops | bytes accessed | tf_op | source)
XLA Modules:
  0.0 181.3 jit_solution(5398701637346977469)
XLA Ops:
  3.0 2.3 %multiply_convert_fusion = bf16[768,512]{1,0:T(8,128)(2,1)} fusion(pred[768,256]{1,0:T(32,128)(4,1)S(1)} %bitcast_compare_fusion, f32[768]{0:T(1024)S(1)} %mul.247, bf16[256,2048]{1,0:T(8,128)(2,1)} %param.14, s32[]{:T(128)S(6)} %select_n.34), kind=kOutput, calls=%fused_computation.36 | convolution fusion | flops 202113024 | bytes 1248260 | tf_op jit(solution)/shard_map/dot_general | solution.py:140
  5.3 7.3 %all-to-all-start.1 = ((bf16[8,96,512]{2,1,0:T(8,128)(2,1)}), bf16[8,96,512]{2,1,0:T(8,128)(2,1)S(1)}, u32[]{:S(2)}, u32[]{:S(2)}) async-start(bf16[8,96,512]{2,1,0:T(8,128)(2,1)} %bitcast.100), calls=%async_computation.1 | async-start | bytes 1572864 | tf_op jit(solution)/shard_map/all_to_all | solution.py:39
  13.5 2.3 %convolution_convert_fusion.1 = bf16[768,512]{1,0:T(8,128)(2,1)} fusion(pred[768,256]{1,0:T(32,128)(4,1)} %copy-done.12, f32[512]{0:T(512)S(1)} %dynamic_slice.34, f32[256]{0:T(256)S(1)} %get-tuple-element.23, bf16[256,2048]{1,0:T(8,128)(2,1)S(1)} %copy-done.5, s32[]{:T(128)S(6)} %select_n.34), kind=kOutput, calls=%fused_computation.37 | convolution fusion | flops 202244096 | bytes 1248260 | tf_op jit(solution)/shard_map/dot_general | solution.py:139
  15.8 16.9 %all-to-all-done.1 = bf16[8,96,512]{2,1,0:T(8,128)(2,1)S(1)} async-done(((bf16[8,96,512]{2,1,0:T(8,128)(2,1)}), bf16[8,96,512]{2,1,0:T(8,128)(2,1)S(1)}, u32[]{:S(2)}, u32[]{:S(2)}) %all-to-all-start.1) | async-done | bytes 786464 | tf_op jit(solution)/shard_map/all_to_all | solution.py:39
  32.8 3.6 %all-to-all-start = ((bf16[8,96,512]{2,1,0:T(8,128)(2,1)}), bf16[8,96,512]{2,1,0:T(8,128)(2,1)S(1)}, u32[]{:S(2)}, u32[]{:S(2)}) async-start(bf16[8,96,512]{2,1,0:T(8,128)(2,1)} %bitcast.101), calls=%async_computation | async-start | bytes 1572864 | tf_op jit(solution)/shard_map/all_to_all | solution.py:39
  38.6 1.5 collective-permute-start.10
  40.1 16.6 %all-to-all-done = bf16[8,96,512]{2,1,0:T(8,128)(2,1)S(1)} async-done(((bf16[8,96,512]{2,1,0:T(8,128)(2,1)}), bf16[8,96,512]{2,1,0:T(8,128)(2,1)S(1)}, u32[]{:S(2)}, u32[]{:S(2)}) %all-to-all-start) | async-done | bytes 786464 | tf_op jit(solution)/shard_map/all_to_all | solution.py:39
  56.8 1.6 collective-permute-start.1
  59.3 1.0 constant_dynamic-update-slice_fusion.7
  60.8 1.6 collective-permute-start.7
  62.4 1.0 constant_dynamic-update-slice_fusion.6
  64.1 1.0 constant_dynamic-update-slice_fusion.5
  65.1 3.7 %collective-permute-done.1 = bf16[384,512]{1,0:T(8,128)(2,1)S(1)} collective-permute-done((bf16[384,512]{1,0:T(8,128)(2,1)S(1)}, bf16[384,512]{1,0:T(8,128)(2,1)S(1)}, u32[]{:S(2)}, u32[]{:S(2)}) %collective-permute-start.1) | collective-permute-done | bytes 393248 | tf_op jit(solution)/shard_map/ppermute | solution.py:35
  68.9 8.4 %collective-permute-done.4 = bf16[384,512]{1,0:T(8,128)(2,1)S(1)} collective-permute-done((bf16[384,512]{1,0:T(8,128)(2,1)S(1)}, bf16[384,512]{1,0:T(8,128)(2,1)S(1)}, u32[]{:S(2)}, u32[]{:S(2)}) %collective-permute-start.4) | collective-permute-done | bytes 393248 | tf_op jit(solution)/shard_map/ppermute | solution.py:35
  77.3 6.1 %collective-permute-done.7 = bf16[384,512]{1,0:T(8,128)(2,1)S(1)} collective-permute-done((bf16[384,512]{1,0:T(8,128)(2,1)S(1)}, bf16[384,512]{1,0:T(8,128)(2,1)S(1)}, u32[]{:S(2)}, u32[]{:S(2)}) %collective-permute-start.7) | collective-permute-done | bytes 393248 | tf_op jit(solution)/shard_map/ppermute | solution.py:35
  84.2 1.2 copy-done.10
  89.1 1.3 select_convert_fusion.1
  91.4 1.0 fusion.20
  92.5 1.3 select_convert_fusion
  93.9 1.0 fusion.18
  94.9 1.0 add_convert_fusion
  96.1 1.0 add_convert_fusion.1
  98.6 1.6 collective-permute-start.17
  102.2 8.5 %collective-permute-done.17 = bf16[384,512]{1,0:T(8,128)(2,1)S(1)} collective-permute-done((bf16[384,512]{1,0:T(8,128)(2,1)S(1)}, bf16[384,512]{1,0:T(8,128)(2,1)S(1)}, u32[]{:S(2)}, u32[]{:S(2)}) %collective-permute-start.17) | collective-permute-done | bytes 393248 | tf_op jit(solution)/shard_map/ppermute | solution.py:35
  111.7 4.9 %all-to-all-start.3 = ((bf16[8,48,512]{2,1,0:T(8,128)(2,1)}), bf16[8,48,512]{2,1,0:T(8,128)(2,1)}, u32[]{:S(2)}, u32[]{:S(2)}) async-start(bf16[8,48,512]{2,1,0:T(8,128)(2,1)} %bitcast.18), calls=%async_computation.3 | async-start | bytes 786432 | tf_op jit(solution)/shard_map/all_to_all | solution.py:39
  117.1 4.5 %fusion.33 = f32[384,2048]{1,0:T(8,128)} fusion(bf16[384,2048]{1,0:T(8,128)(2,1)} %copy-done.7, f32[384,384]{1,0:T(8,128)} %copy-done.18, f32[384,384]{1,0:T(8,128)} %copy-done.19), kind=kOutput, calls=%fused_computation.73 | convolution fusion | flops 605454336 | bytes 5898240 | tf_op jit(solution)/shard_map/dot_general | solution.py:22
  121.6 2.2 %add_convert_fusion.8 = bf16[384,512]{1,0:T(8,128)(2,1)} fusion(bf16[384,512]{1,0:T(8,128)(2,1)} %collective-permute-done.14, bf16[384,512]{1,0:T(8,128)(2,1)} %collective-permute-done.12, bf16[384,2048]{1,0:T(8,128)(2,1)} %copy-done.11, s32[]{:T(128)S(6)} %select_n.34), kind=kLoop, calls=%fused_computation.53 | loop fusion | flops 1572864 | bytes 1572868 | tf_op jit(solution)/shard_map/convert_element_type | solution.py:71
  123.8 3.8 %all-to-all-done.3 = bf16[8,48,512]{2,1,0:T(8,128)(2,1)} async-done(((bf16[8,48,512]{2,1,0:T(8,128)(2,1)}), bf16[8,48,512]{2,1,0:T(8,128)(2,1)}, u32[]{:S(2)}, u32[]{:S(2)}) %all-to-all-start.3) | async-done | bytes 393248 | tf_op jit(solution)/shard_map/all_to_all | solution.py:39
  127.6 4.1 %all-to-all-start.2 = ((bf16[8,48,512]{2,1,0:T(8,128)(2,1)}), bf16[8,48,512]{2,1,0:T(8,128)(2,1)}, u32[]{:S(2)}, u32[]{:S(2)}) async-start(bf16[8,48,512]{2,1,0:T(8,128)(2,1)} %bitcast.16), calls=%async_computation.2 | async-start | bytes 786432 | tf_op jit(solution)/shard_map/all_to_all | solution.py:39
  131.8 4.0 %fusion.92 = f32[2048,384]{1,0:T(8,128)} fusion(bf16[384,2048]{1,0:T(8,128)(2,1)S(1)} %constant_dynamic-update-slice_fusion.8, bf16[384,384]{1,0:T(8,128)(2,1)} %copy-done.17), kind=kOutput, calls=%fused_computation.173 | convolution fusion | flops 603979776 | bytes 5013504 | tf_op jit(solution)/shard_map/dot_general | solution.py:22
  135.8 2.3 %fusion.2 = bf16[1,384,2048]{2,1,0:T(8,128)(2,1)} fusion(f32[384,2048]{1,0:T(8,128)S(1)} %copy-done.2, bf16[384,2048]{1,0:T(8,128)(2,1)S(1)} %copy-done.9, f32[384,384]{1,0:T(8,128)S(1)} %copy-done.21, f32[384,384]{1,0:T(8,128)S(1)} %copy-done.23), kind=kOutput, calls=%fused_computation.10 | convolution fusion | flops 607027200 | bytes 7471104 | tf_op jit(solution)/shard_map/dot_general | solution.py:22
  138.1 2.1 %convolution_bitcast_fusion = f32[256,512]{1,0:T(8,128)} fusion(bf16[8,48,512]{2,1,0:T(8,128)(2,1)} %all-to-all-done.3, pred[8,96,256]{2,1,0:T(8,128)(4,1)S(1)} %copy-done.26), kind=kOutput, calls=%fused_computation.38 | convolution fusion | flops 100663296 | bytes 1015808 | tf_op jit(solution)/shard_map/dot_general | solution.py:22
  140.2 2.7 %all-to-all-done.2 = bf16[8,48,512]{2,1,0:T(8,128)(2,1)} async-done(((bf16[8,48,512]{2,1,0:T(8,128)(2,1)}), bf16[8,48,512]{2,1,0:T(8,128)(2,1)}, u32[]{:S(2)}, u32[]{:S(2)}) %all-to-all-start.2) | async-done | bytes 393248 | tf_op jit(solution)/shard_map/all_to_all | solution.py:39
  143.1 1.7 constant_dynamic-update-slice_fusion.3
  144.8 1.6 collective-permute-start.19
  146.3 3.8 %fusion.1 = bf16[1,2048,384]{2,1,0:T(8,128)(2,1)} fusion(f32[2048,384]{1,0:T(8,128)S(1)} %copy-done.1, bf16[384,2048]{1,0:T(8,128)(2,1)} %copy-done.3, bf16[384,384]{1,0:T(8,128)(2,1)} %copy-done.16), kind=kOutput, calls=%fused_computation.9 | convolution fusion | flops 605552640 | bytes 6586368 | tf_op jit(solution)/shard_map/dot_general | solution.py:22
  150.2 1.1 collective-permute-done.19
  151.2 2.8 %fusion.91 = f32[2048,384]{1,0:T(8,128)} fusion(bf16[384,2048]{1,0:T(8,128)(2,1)S(1)} %constant_dynamic-update-slice_fusion.8, bf16[384,384]{1,0:T(8,128)(2,1)S(1)} %copy-done.15), kind=kOutput, calls=%fused_computation.172 | convolution fusion | flops 603979776 | bytes 5013504 | tf_op jit(solution)/shard_map/dot_general | solution.py:22
  154.2 1.1 copy-done.6
  156.5 1.4 convolution_convert_fusion
  157.9 1.1 fusion.88
  159.0 5.1 %all-to-all-start.4 = ((bf16[8,256,128]{2,1,0:T(8,128)(2,1)}), bf16[8,256,128]{2,1,0:T(8,128)(2,1)}, u32[]{:S(2)}, u32[]{:S(2)}) async-start(bf16[8,256,128]{2,1,0:T(8,128)(2,1)} %bitcast.112), calls=%async_computation.4 | async-start | bytes 1048576 | tf_op jit(solution)/shard_map/all_to_all | solution.py:39
  164.1 1.1 fusion.65
  165.3 1.3 collective-permute-start.21
  166.6 4.2 %fusion = bf16[1,2048,384]{2,1,0:T(8,128)(2,1)} fusion(f32[2048,384]{1,0:T(8,128)} %fusion.91, bf16[384,2048]{1,0:T(8,128)(2,1)S(1)} %copy-done.4, bf16[384,384]{1,0:T(8,128)(2,1)S(1)} %get-tuple-element.9), kind=kOutput, calls=%fused_computation.8 | convolution fusion | flops 605552640 | bytes 6586368 | tf_op jit(solution)/shard_map/dot_general | solution.py:22
  170.8 1.2 collective-permute-done.21
  173.6 5.9 %all-to-all-done.4 = bf16[8,256,128]{2,1,0:T(8,128)(2,1)} async-done(((bf16[8,256,128]{2,1,0:T(8,128)(2,1)}), bf16[8,256,128]{2,1,0:T(8,128)(2,1)}, u32[]{:S(2)}, u32[]{:S(2)}) %all-to-all-start.4) | async-done | bytes 524320 | tf_op jit(solution)/shard_map/all_to_all | solution.py:39
  179.5 1.8 convert_reduce_fusion
  (168 shorter events, 21.4 us)
Async XLA Ops:
  0.6 85.9 %copy-start = (bf16[1,2048,384]{2,1,0:T(8,128)(2,1)S(1)}, bf16[1,2048,384]{2,1,0:T(8,128)(2,1)}, u32[]{:S(2)}) copy-start(bf16[1,2048,384]{2,1,0:T(8,128)(2,1)} %param.19) | copy-start | bytes 4718596
  1.5 11.1 %copy-start.29 = (f32[2048]{0:T(1024)S(1)}, f32[2048]{0:T(1024)}, u32[]{:S(2)}) copy-start(f32[2048]{0:T(1024)} %param.16) | copy-start | bytes 24580
  1.5 11.2 %copy-start.5 = (bf16[256,2048]{1,0:T(8,128)(2,1)S(1)}, bf16[256,2048]{1,0:T(8,128)(2,1)}, u32[]{:S(2)}) copy-start(bf16[256,2048]{1,0:T(8,128)(2,1)} %param.15) | copy-start | bytes 3145732
  3.0 2.3 %copy-start.12 = (pred[768,256]{1,0:T(32,128)(4,1)}, pred[768,256]{1,0:T(32,128)(4,1)S(1)}, u32[]{:S(2)}) copy-start(pred[768,256]{1,0:T(32,128)(4,1)S(1)} %bitcast_compare_fusion) | copy-start | bytes 589828
  5.3 27.5 %all-to-all-start.1 = ((bf16[8,96,512]{2,1,0:T(8,128)(2,1)}), bf16[8,96,512]{2,1,0:T(8,128)(2,1)S(1)}, u32[]{:S(2)}, u32[]{:S(2)}) async-start(bf16[8,96,512]{2,1,0:T(8,128)(2,1)} %bitcast.100), calls=%async_computation.1 | async-start | bytes 1572864 | tf_op jit(solution)/shard_map/all_to_all | solution.py:39
  13.0 23.4 %copy-start.24 = (bf16[256,128]{1,0:T(8,128)(2,1)S(1)}, bf16[256,128]{1,0:T(8,128)(2,1)}, u32[]{:S(2)}) copy-start(bf16[256,128]{1,0:T(8,128)(2,1)} %param.23) | copy-start | bytes 196612
  32.8 24.0 %all-to-all-start = ((bf16[8,96,512]{2,1,0:T(8,128)(2,1)}), bf16[8,96,512]{2,1,0:T(8,128)(2,1)S(1)}, u32[]{:S(2)}, u32[]{:S(2)}) async-start(bf16[8,96,512]{2,1,0:T(8,128)(2,1)} %bitcast.101), calls=%async_computation | async-start | bytes 1572864 | tf_op jit(solution)/shard_map/all_to_all | solution.py:39
  38.6 24.9 %collective-permute-start.10 = (bf16[384,512]{1,0:T(8,128)(2,1)}, bf16[384,512]{1,0:T(8,128)(2,1)}, u32[]{:S(2)}, u32[]{:S(2)}) collective-permute-start(bf16[384,512]{1,0:T(8,128)(2,1)} %bitcast.12), channel_id=1, source_target_pairs={{0,2},{1,3},{2,0},{3,1},{4,6},{5,7},{6,4},{7,5},{8,10},{9,11},{10,... | collective-permute-start | bytes 1179656 | tf_op jit(solution)/shard_map/ppermute | solution.py:35
  40.1 20.7 %collective-permute-start.9 = (bf16[384,512]{1,0:T(8,128)(2,1)}, bf16[384,512]{1,0:T(8,128)(2,1)}, u32[]{:S(2)}, u32[]{:S(2)}) collective-permute-start(bf16[384,512]{1,0:T(8,128)(2,1)} %bitcast.12), channel_id=1, source_target_pairs={{0,1},{1,0},{2,3},{3,2},{4,5},{5,4},{6,7},{7,6},{8,9},{9,8},{10,11... | collective-permute-start | bytes 1179656 | tf_op jit(solution)/shard_map/ppermute | solution.py:35
  56.8 12.1 %collective-permute-start.1 = (bf16[384,512]{1,0:T(8,128)(2,1)S(1)}, bf16[384,512]{1,0:T(8,128)(2,1)S(1)}, u32[]{:S(2)}, u32[]{:S(2)}) collective-permute-start(bf16[384,512]{1,0:T(8,128)(2,1)S(1)} %bitcast.108), channel_id=1, source_target_pairs={{0,2},{1,3},{2,0},{3,1},{4,6},{5,7},{6,4},{7,5},{8,10},{9,11},{10,... | collective-permute-start | bytes 1179656 | tf_op jit(solution)/shard_map/ppermute | solution.py:35
  58.3 4.1 %collective-permute-start = (bf16[384,512]{1,0:T(8,128)(2,1)S(1)}, bf16[384,512]{1,0:T(8,128)(2,1)S(1)}, u32[]{:S(2)}, u32[]{:S(2)}) collective-permute-start(bf16[384,512]{1,0:T(8,128)(2,1)S(1)} %bitcast.109), channel_id=1, source_target_pairs={{0,1},{1,0},{2,3},{3,2},{4,5},{5,4},{6,7},{7,6},{8,9},{9,8},{10,11... | collective-permute-start | bytes 1179656 | tf_op jit(solution)/shard_map/ppermute | solution.py:35
  58.3 18.9 %collective-permute-start.4 = (bf16[384,512]{1,0:T(8,128)(2,1)S(1)}, bf16[384,512]{1,0:T(8,128)(2,1)S(1)}, u32[]{:S(2)}, u32[]{:S(2)}) collective-permute-start(bf16[384,512]{1,0:T(8,128)(2,1)S(1)} %bitcast.102), channel_id=1, source_target_pairs={{0,2},{1,3},{2,0},{3,1},{4,6},{5,7},{6,4},{7,5},{8,10},{9,11},{10,... | collective-permute-start | bytes 1179656 | tf_op jit(solution)/shard_map/ppermute | solution.py:35
  60.8 22.6 %collective-permute-start.7 = (bf16[384,512]{1,0:T(8,128)(2,1)S(1)}, bf16[384,512]{1,0:T(8,128)(2,1)S(1)}, u32[]{:S(2)}, u32[]{:S(2)}) collective-permute-start(bf16[384,512]{1,0:T(8,128)(2,1)S(1)} %bitcast.106), channel_id=1, source_target_pairs={{0,2},{1,3},{2,0},{3,1},{4,6},{5,7},{6,4},{7,5},{8,10},{9,11},{10,... | collective-permute-start | bytes 1179656 | tf_op jit(solution)/shard_map/ppermute | solution.py:35
  62.4 21.0 %collective-permute-start.6 = (bf16[384,512]{1,0:T(8,128)(2,1)S(1)}, bf16[384,512]{1,0:T(8,128)(2,1)S(1)}, u32[]{:S(2)}, u32[]{:S(2)}) collective-permute-start(bf16[384,512]{1,0:T(8,128)(2,1)S(1)} %bitcast.107), channel_id=1, source_target_pairs={{0,1},{1,0},{2,3},{3,2},{4,5},{5,4},{6,7},{7,6},{8,9},{9,8},{10,11... | collective-permute-start | bytes 1179656 | tf_op jit(solution)/shard_map/ppermute | solution.py:35
  63.5 20.5 %collective-permute-start.3 = (bf16[384,512]{1,0:T(8,128)(2,1)S(1)}, bf16[384,512]{1,0:T(8,128)(2,1)S(1)}, u32[]{:S(2)}, u32[]{:S(2)}) collective-permute-start(bf16[384,512]{1,0:T(8,128)(2,1)S(1)} %bitcast.104), channel_id=1, source_target_pairs={{0,1},{1,0},{2,3},{3,2},{4,5},{5,4},{6,7},{7,6},{8,9},{9,8},{10,11... | collective-permute-start | bytes 1179656 | tf_op jit(solution)/shard_map/ppermute | solution.py:35
  68.8 23.6 %collective-permute-start.11 = (bf16[384,512]{1,0:T(8,128)(2,1)}, bf16[384,512]{1,0:T(8,128)(2,1)S(1)}, u32[]{:S(2)}, u32[]{:S(2)}) collective-permute-start(bf16[384,512]{1,0:T(8,128)(2,1)} %collective-permute-done.10), channel_id=1, source_target_pairs={{0,1},{1,0},{2,3},{3,2},{4,5},{5,4},{6,7},{7,6},{8,9},{9,8},{10,11... | collective-permute-start | bytes 1179656 | tf_op jit(solution)/shard_map/ppermute | solution.py:35
  77.3 6.9 %collective-permute-start.2 = (bf16[384,512]{1,0:T(8,128)(2,1)S(1)}, bf16[384,512]{1,0:T(8,128)(2,1)S(1)}, u32[]{:S(2)}, u32[]{:S(2)}) collective-permute-start(bf16[384,512]{1,0:T(8,128)(2,1)S(1)} %collective-permute-done.1), channel_id=1, source_target_pairs={{0,1},{1,0},{2,3},{3,2},{4,5},{5,4},{6,7},{7,6},{8,9},{9,8},{10,11... | collective-permute-start | bytes 1179656 | tf_op jit(solution)/shard_map/ppermute | solution.py:35
  83.4 5.2 %collective-permute-start.5 = (bf16[384,512]{1,0:T(8,128)(2,1)S(1)}, bf16[384,512]{1,0:T(8,128)(2,1)S(1)}, u32[]{:S(2)}, u32[]{:S(2)}) collective-permute-start(bf16[384,512]{1,0:T(8,128)(2,1)S(1)} %collective-permute-done.4), channel_id=1, source_target_pairs={{0,1},{1,0},{2,3},{3,2},{4,5},{5,4},{6,7},{7,6},{8,9},{9,8},{10,11... | collective-permute-start | bytes 1179656 | tf_op jit(solution)/shard_map/ppermute | solution.py:35
  83.4 4.1 %collective-permute-start.8 = (bf16[384,512]{1,0:T(8,128)(2,1)S(1)}, bf16[384,512]{1,0:T(8,128)(2,1)S(1)}, u32[]{:S(2)}, u32[]{:S(2)}) collective-permute-start(bf16[384,512]{1,0:T(8,128)(2,1)S(1)} %collective-permute-done.7), channel_id=1, source_target_pairs={{0,1},{1,0},{2,3},{3,2},{4,5},{5,4},{6,7},{7,6},{8,9},{9,8},{10,11... | collective-permute-start | bytes 1179656 | tf_op jit(solution)/shard_map/ppermute | solution.py:35
  86.5 2.1 %copy-start.20 = (f32[384,384]{1,0:T(8,128)}, f32[384,384]{1,0:T(8,128)S(1)}, u32[]{:S(2)}) copy-start(f32[384,384]{1,0:T(8,128)S(1)} %fusion.12) | copy-start | bytes 1769476
  88.6 3.9 %copy-start.18 = (f32[384,384]{1,0:T(8,128)}, f32[384,384]{1,0:T(8,128)S(1)}, u32[]{:S(2)}) copy-start(f32[384,384]{1,0:T(8,128)S(1)} %fusion.10) | copy-start | bytes 1769476
  90.4 5.7 %copy-start.16 = (bf16[384,384]{1,0:T(8,128)(2,1)}, bf16[384,384]{1,0:T(8,128)(2,1)S(1)}, u32[]{:S(2)}) copy-start(bf16[384,384]{1,0:T(8,128)(2,1)S(1)} %get-tuple-element.8) | copy-start | bytes 884740
  96.0 2.5 %collective-permute-start.16 = (bf16[384,512]{1,0:T(8,128)(2,1)S(1)}, bf16[384,512]{1,0:T(8,128)(2,1)S(1)}, u32[]{:S(2)}, u32[]{:S(2)}) collective-permute-start(bf16[384,512]{1,0:T(8,128)(2,1)S(1)} %get-tuple-element.15), channel_id=1, source_target_pairs={{0,1},{1,0},{2,3},{3,2},{4,5},{5,4},{6,7},{7,6},{8,9},{9,8},{10,11... | collective-permute-start | bytes 1179656 | tf_op jit(solution)/shard_map/ppermute | solution.py:35
  97.1 4.5 %copy-start.11 = (bf16[384,2048]{1,0:T(8,128)(2,1)}, bf16[384,2048]{1,0:T(8,128)(2,1)S(1)}, u32[]{:S(2)}) copy-start(bf16[384,2048]{1,0:T(8,128)(2,1)S(1)} %add_convert_fusion.1) | copy-start | bytes 4718596
  97.1 3.1 %copy-start.32 = (f32[256]{0:T(256)S(1)}, f32[256]{0:T(256)}, u32[]{:S(2)}) copy-start(f32[256]{0:T(256)} %convert_reduce_fusion.1) | copy-start | bytes 3076
  97.1 3.1 %copy-start.25 = (bf16[256,128]{1,0:T(8,128)(2,1)S(1)}, bf16[256,128]{1,0:T(8,128)(2,1)}, u32[]{:S(2)}) copy-start(bf16[256,128]{1,0:T(8,128)(2,1)} %param.23) | copy-start | bytes 196612
  98.0 2.7 %collective-permute-start.13 = (bf16[384,512]{1,0:T(8,128)(2,1)S(1)}, bf16[384,512]{1,0:T(8,128)(2,1)S(1)}, u32[]{:S(2)}, u32[]{:S(2)}) collective-permute-start(bf16[384,512]{1,0:T(8,128)(2,1)S(1)} %get-tuple-element.13), channel_id=1, source_target_pairs={{0,1},{1,0},{2,3},{3,2},{4,5},{5,4},{6,7},{7,6},{8,9},{9,8},{10,11... | collective-permute-start | bytes 1179656 | tf_op jit(solution)/shard_map/ppermute | solution.py:35
  98.5 3.7 %collective-permute-start.15 = (bf16[384,512]{1,0:T(8,128)(2,1)S(1)}, bf16[384,512]{1,0:T(8,128)(2,1)S(1)}, u32[]{:S(2)}, u32[]{:S(2)}) collective-permute-start(bf16[384,512]{1,0:T(8,128)(2,1)S(1)} %get-tuple-element.14), channel_id=1, source_target_pairs={{0,1},{1,0},{2,3},{3,2},{4,5},{5,4},{6,7},{7,6},{8,9},{9,8},{10,11... | collective-permute-start | bytes 1179656 | tf_op jit(solution)/shard_map/ppermute | solution.py:35
  98.6 12.1 %collective-permute-start.17 = (bf16[384,512]{1,0:T(8,128)(2,1)S(1)}, bf16[384,512]{1,0:T(8,128)(2,1)S(1)}, u32[]{:S(2)}, u32[]{:S(2)}) collective-permute-start(bf16[384,512]{1,0:T(8,128)(2,1)S(1)} %add_convert_fusion.6), channel_id=1, source_target_pairs={{0,2},{1,3},{2,0},{3,1},{4,6},{5,7},{6,4},{7,5},{8,10},{9,11},{10,... | collective-permute-start | bytes 1179656 | tf_op jit(solution)/shard_map/ppermute | solution.py:35
  100.4 16.7 %copy-start.30 = (f32[31,128]{1,0:T(8,128)S(1)}, f32[31,128]{1,0:T(8,128)}, u32[]{:S(2)}) copy-start(f32[31,128]{1,0:T(8,128)} %param.25) | copy-start | bytes 47620
  100.4 21.2 %collective-permute-start.12 = (bf16[384,512]{1,0:T(8,128)(2,1)}, bf16[384,512]{1,0:T(8,128)(2,1)}, u32[]{:S(2)}, u32[]{:S(2)}) collective-permute-start(bf16[384,512]{1,0:T(8,128)(2,1)} %get-tuple-element.12), channel_id=1, source_target_pairs={{0,1},{1,0},{2,3},{3,2},{4,5},{5,4},{6,7},{7,6},{8,9},{9,8},{10,11... | collective-permute-start | bytes 1179656 | tf_op jit(solution)/shard_map/ppermute | solution.py:35
  101.6 20.1 %collective-permute-start.14 = (bf16[384,512]{1,0:T(8,128)(2,1)}, bf16[384,512]{1,0:T(8,128)(2,1)}, u32[]{:S(2)}, u32[]{:S(2)}) collective-permute-start(bf16[384,512]{1,0:T(8,128)(2,1)} %add_convert_fusion.9), channel_id=1, source_target_pairs={{0,2},{1,3},{2,0},{3,1},{4,6},{5,7},{6,4},{7,5},{8,10},{9,11},{10,... | collective-permute-start | bytes 1179656 | tf_op jit(solution)/shard_map/ppermute | solution.py:35
  111.7 16.0 %all-to-all-start.3 = ((bf16[8,48,512]{2,1,0:T(8,128)(2,1)}), bf16[8,48,512]{2,1,0:T(8,128)(2,1)}, u32[]{:S(2)}, u32[]{:S(2)}) async-start(bf16[8,48,512]{2,1,0:T(8,128)(2,1)} %bitcast.18), calls=%async_computation.3 | async-start | bytes 786432 | tf_op jit(solution)/shard_map/all_to_all | solution.py:39
  127.6 15.3 %all-to-all-start.2 = ((bf16[8,48,512]{2,1,0:T(8,128)(2,1)}), bf16[8,48,512]{2,1,0:T(8,128)(2,1)}, u32[]{:S(2)}, u32[]{:S(2)}) async-start(bf16[8,48,512]{2,1,0:T(8,128)(2,1)} %bitcast.16), calls=%async_computation.2 | async-start | bytes 786432 | tf_op jit(solution)/shard_map/all_to_all | solution.py:39
  131.8 4.0 %copy-start.2 = (f32[384,2048]{1,0:T(8,128)S(1)}, f32[384,2048]{1,0:T(8,128)}, u32[]{:S(2)}) copy-start(f32[384,2048]{1,0:T(8,128)} %fusion.33) | copy-start | bytes 9437188
  131.8 4.0 %copy-start.9 = (bf16[384,2048]{1,0:T(8,128)(2,1)S(1)}, bf16[384,2048]{1,0:T(8,128)(2,1)}, u32[]{:S(2)}) copy-start(bf16[384,2048]{1,0:T(8,128)(2,1)} %copy-done.8) | copy-start | bytes 4718596
  131.8 4.0 %copy-start.21 = (f32[384,384]{1,0:T(8,128)S(1)}, f32[384,384]{1,0:T(8,128)}, u32[]{:S(2)}) copy-start(f32[384,384]{1,0:T(8,128)} %copy-done.20) | copy-start | bytes 1769476
  131.8 4.0 %copy-start.23 = (f32[384,384]{1,0:T(8,128)S(1)}, f32[384,384]{1,0:T(8,128)}, u32[]{:S(2)}) copy-start(f32[384,384]{1,0:T(8,128)} %copy-done.22) | copy-start | bytes 1769476
  135.8 2.3 %copy-start.26 = (pred[8,96,256]{2,1,0:T(8,128)(4,1)S(1)}, pred[8,96,256]{2,1,0:T(8,128)(4,1)}, u32[]{:S(2)}) copy-start(pred[8,96,256]{2,1,0:T(8,128)(4,1)} %iota_compare_fusion) | copy-start | bytes 589828
  142.9 3.4 %copy-start.1 = (f32[2048,384]{1,0:T(8,128)S(1)}, f32[2048,384]{1,0:T(8,128)}, u32[]{:S(2)}) copy-start(f32[2048,384]{1,0:T(8,128)} %fusion.92) | copy-start | bytes 9437188
  144.8 6.5 %copy-start.15 = (bf16[384,384]{1,0:T(8,128)(2,1)S(1)}, bf16[384,384]{1,0:T(8,128)(2,1)}, u32[]{:S(2)}) copy-start(bf16[384,384]{1,0:T(8,128)(2,1)} %copy-done.14) | copy-start | bytes 884740
  144.8 6.4 %collective-permute-start.19 = (bf16[256,512]{1,0:T(8,128)(2,1)S(1)}, bf16[256,512]{1,0:T(8,128)(2,1)S(1)}, u32[]{:S(2)}, u32[]{:S(2)}) collective-permute-start(bf16[256,512]{1,0:T(8,128)(2,1)S(1)} %get-tuple-element.25), channel_id=1, source_target_pairs={{0,2},{1,3},{2,0},{3,1},{4,6},{5,7},{6,4},{7,5},{8,10},{9,11},{10,... | collective-permute-start | bytes 786440 | tf_op jit(solution)/shard_map/ppermute | solution.py:35
  150.2 3.9 %collective-permute-start.18 = (bf16[256,512]{1,0:T(8,128)(2,1)S(1)}, bf16[256,512]{1,0:T(8,128)(2,1)S(1)}, u32[]{:S(2)}, u32[]{:S(2)}) collective-permute-start(bf16[256,512]{1,0:T(8,128)(2,1)S(1)} %get-tuple-element.25), channel_id=1, source_target_pairs={{0,1},{1,0},{2,3},{3,2},{4,5},{5,4},{6,7},{7,6},{8,9},{9,8},{10,11... | collective-permute-start | bytes 786440 | tf_op jit(solution)/shard_map/ppermute | solution.py:35
  151.2 2.9 %collective-permute-start.20 = (bf16[256,512]{1,0:T(8,128)(2,1)S(1)}, bf16[256,512]{1,0:T(8,128)(2,1)S(1)}, u32[]{:S(2)}, u32[]{:S(2)}) collective-permute-start(bf16[256,512]{1,0:T(8,128)(2,1)S(1)} %collective-permute-done.19), channel_id=1, source_target_pairs={{0,1},{1,0},{2,3},{3,2},{4,5},{5,4},{6,7},{7,6},{8,9},{9,8},{10,11... | collective-permute-start | bytes 786440 | tf_op jit(solution)/shard_map/ppermute | solution.py:35
  157.9 8.7 %copy-start.4 = (bf16[384,2048]{1,0:T(8,128)(2,1)S(1)}, bf16[384,2048]{1,0:T(8,128)(2,1)}, u32[]{:S(2)}) copy-start(bf16[384,2048]{1,0:T(8,128)(2,1)} %copy-done.3) | copy-start | bytes 4718596
  159.0 20.5 %all-to-all-start.4 = ((bf16[8,256,128]{2,1,0:T(8,128)(2,1)}), bf16[8,256,128]{2,1,0:T(8,128)(2,1)}, u32[]{:S(2)}, u32[]{:S(2)}) async-start(bf16[8,256,128]{2,1,0:T(8,128)(2,1)} %bitcast.112), calls=%async_computation.4 | async-start | bytes 1048576 | tf_op jit(solution)/shard_map/all_to_all | solution.py:39
  165.2 6.8 %copy-start.37 = (pred[8,36]{0,1:T(8,128)(4,1)S(1)}, pred[8,36]{0,1:T(8,128)(4,1)}, u32[]{:S(2)}) copy-start(pred[8,36]{0,1:T(8,128)(4,1)} %constant.57) | copy-start | bytes 868
  165.3 6.7 %collective-permute-start.21 = (f32[30,128]{1,0:T(8,128)S(1)}, f32[30,128]{1,0:T(8,128)S(1)}, u32[]{:S(2)}, u32[]{:S(2)}) collective-permute-start(f32[30,128]{1,0:T(8,128)S(1)} %slice.48), channel_id=1, source_target_pairs={{4,0},{8,4},{12,8},{16,12},{20,16},{24,20},{28,24},{5,1},{9,5},{13... | collective-permute-start | bytes 46088 | tf_op jit(solution)/shard_map/ppermute | solution.py:18
  (17 other events, 20.1 us)
